TPU v7x, 32 devices: a whole 2x2x4 slice. The times are simulated.
32 devices in a mesh: fs: 8 (over z, y), tp: 4 (over x, core).
Axes of the slice: x: 2, y: 2, z: 4, core: 2. Of those that a mesh axis runs over, the one named last changes fastest.
Arguments:
- tokens: bfloat16 [8192, 2048], P('fs', 'tp'), may hold values from -6 to 6
- mixer_gain: float32 [2048], replicated, may hold values from 0.1 to 1.9
- conv_taps: bfloat16 [3, 1024], replicated, may hold values from -3.5 to 3.5
- outer_weight: bfloat16 [2048, 1024], P('fs', 'tp'), may hold values from -0.125 to 0.125
- inner_weight: bfloat16 [2048, 1024], P('fs', 'tp'), may hold values from -0.125 to 0.125
- value_weight: bfloat16 [2048, 1024], P('fs', 'tp'), may hold values from -0.125 to 0.125
- merge_weight: bfloat16 [1024, 2048], P('tp', 'fs'), may hold values from -0.25 to 0.25
- merge_gain: float32 [2048], replicated, may hold values from 0.1 to 1.9
- channel_gain: float32 [2048], replicated, may hold values from 0.1 to 1.9
- gate_weight: bfloat16 [2048, 5632], P('fs', 'tp'), may hold values from -0.125 to 0.125
- up_weight: bfloat16 [2048, 5632], P('fs', 'tp'), may hold values from -0.125 to 0.125
- down_weight: bfloat16 [5632, 2048], P('tp', 'fs'), may hold values from -0.109375 to 0.109375
- output_gain: float32 [2048], replicated, may hold values from 0.1 to 1.9
Outputs:
- layer_out: bfloat16 [8192, 2048], P('fs', 'tp')
All inputs are finite; a program needn't handle non-finite values.
Results may differ from a plain program's by a relative error of at most 0.018.
Values may be sent and summed in bfloat16 or wider, within the bound.
A program may use at most 128 MiB of HBM per device.

v0:
```python
import jax
import jax.numpy as jnp
from jax import lax
from jax.experimental import pallas as pl
from jax.experimental.pallas import tpu as pltpu
from jax.sharding import PartitionSpec as P

HEAD_DIM = 128
EPS = 1e-06
MESH = pl.DeviceIdType.MESH
F32 = jnp.float32
BF16 = jnp.bfloat16
MIX, FEED, DOWN = (0, 1, 2, 3), (4, 5), (6, 7)


def layer_kernel(
    n, nt, tokens, mixer_gain, conv_taps, outer_w, inner_w, value_w, merge_w, merge_gain,
    channel_gain, gate_w, up_w, down_w, output_gain,
    out,
    toks, nrm, full_outer, full_inner, full_value, full_merge, full_gate, full_up, full_down,
    outer_s, sig, mixed, part, mrecv, msum, merged, hidden, drecv, sq_own, sq_in,
    ring_send, ring_recv, tok_send, tok_recv, rs_send, rs_recv, ag_send, ag_recv, dn_send, dn_recv,
    sq_send, sq_recv,
):
    f, t = lax.axis_index("fs"), lax.axis_index("tp")
    half = n // 2
    odd = lax.rem(f, 2)
    pos = (1 - odd) * (f // 2) + odd * (n - 1 - f // 2)
    length, width = tokens.shape
    blk, channels = outer_w.shape
    cols = merge_w.shape[1]
    bps = n // nt
    depth = width * nt
    tile = min(256, length)
    tiles = length // tile

    def owner(p):
        q = lax.rem(p + 2 * n, n)
        high = q // half
        return (1 - high) * (2 * q) + high * (2 * (n - 1 - q) + 1)

    right, left = owner(pos + 1), owner(pos - 1)
    rowed = {0: (outer_w, full_outer), 1: (inner_w, full_inner), 2: (value_w, full_value),
             4: (gate_w, full_gate), 5: (up_w, full_up)}
    piece_m = channels // 2
    piece_d = down_w.shape[0] // 4

    def own_region(w, h):
        if w in rowed:
            return rowed[w][0].at[pl.ds(h * (blk // 2), blk // 2)]
        if w == 3:
            return merge_w.at[pl.ds(h * piece_m, piece_m)]
        return down_w.at[pl.ds((h * 2 + w - 6) * piece_d, piece_d)]

    def region(w, h, p):
        i = owner(p)
        if w in rowed:
            start = pl.multiple_of(i * blk + h * (blk // 2), blk // 2)
            return rowed[w][1].at[pl.ds(start, blk // 2)]
        if w == 3:
            return full_merge.at[i, pl.ds(h * piece_m, piece_m)]
        return full_down.at[i, pl.ds((h * 2 + w - 6) * piece_d, piece_d)]

    def ring_copy(w, h, d, s, first=False):
        dst = region(w, h, pos - s if d == 0 else pos + s)
        return pltpu.make_async_remote_copy(
            src_ref=own_region(w, h) if first else dst,
            dst_ref=dst,
            send_sem=ring_send.at[d, h, w],
            recv_sem=ring_recv.at[d, h, w, s],
            device_id={"fs": right if d == 0 else left},
            device_id_type=MESH,
        )

    def ring_arrive(w, h, d, s):
        got = region(w, h, pos - 1 - s if d == 0 else pos + 1 + s)
        pltpu.make_async_remote_copy(
            src_ref=got, dst_ref=got, send_sem=ring_send.at[d, h, w],
            recv_sem=ring_recv.at[d, h, w, s],
            device_id={"fs": right if d == 0 else left}, device_id_type=MESH,
        ).wait_recv()

    def pieces(ws):
        return [(w, (i + d) % 2, d) for i in (0, 1) for w in ws for d in (0, 1)]

    def ring_open(ws):
        for w, h, d in pieces(ws):
            ring_copy(w, h, d, 0, True).start()

    def pump(ws, s, last=False):
        for w, h, d in pieces(ws):
            if last and h != d:
                continue
            ring_arrive(w, h, d, s - 1)
            ring_copy(w, h, d, s - 1).wait_send()
            ring_copy(w, h, d, s).start()
        for w, h, d in pieces(ws):
            if last and h != d:
                ring_arrive(w, h, d, s - 1)
                ring_copy(w, h, d, s - 1).wait_send()

    def pumps(ws, low, high):
        lax.fori_loop(low, high, lambda s, c: (pump(ws, s), c)[1], 0)

    def ring_close(ws):
        for w in ws:
            for d in (0, 1):
                ring_arrive(w, d, d, half - 1)
                ring_copy(w, d, d, half - 1).wait_send()

    def peer(o):
        return lax.rem(t + o, nt)

    def slab_copy(src, dst, send, recv, o):
        return pltpu.make_async_remote_copy(
            src_ref=src, dst_ref=dst, send_sem=send.at[o - 1], recv_sem=recv.at[o - 1],
            device_id={"tp": peer(o)}, device_id_type=MESH,
        )

    offsets = range(1, nt)
    partner = t + 1 - 2 * lax.rem(t, 2)
    strides = range(2, nt, 2)

    def hop(src, dst, send, recv, i, to):
        return pltpu.make_async_remote_copy(
            src_ref=src, dst_ref=dst, send_sem=send.at[i], recv_sem=recv.at[i],
            device_id={"tp": to}, device_id_type=MESH,
        )

    def gather_open(own, held, send, recv):
        for o in strides:
            hop(own, held.at[t], send, recv, o - 1, peer(o)).start()
        hop(own, held.at[t], send, recv, 0, partner).start()

    def gather_relay(own, held, send, recv):
        for o in strides:
            slab = held.at[peer(nt - o)]
            hop(own, slab, send, recv, o - 1, peer(o)).wait()
            hop(slab, slab, send, recv, o, partner).start()

    def gather_close(own, held, send, recv):
        hop(own, held.at[partner], send, recv, 0, partner).wait()
        for o in strides:
            slab = held.at[lax.rem(partner + nt - o, nt)]
            hop(held.at[peer(nt - o)], slab, send, recv, o, partner).wait()

    tok_args = (tokens, toks, tok_send, tok_recv)
    sum_args = (msum, merged, ag_send, ag_recv)

    barrier = pltpu.get_barrier_semaphore()
    for to in ({"fs": left}, {"fs": right}) + tuple({"tp": peer(o)} for o in offsets):
        pl.semaphore_signal(barrier, inc=1, device_id=to, device_id_type=MESH)
    pl.semaphore_wait(barrier, 2 + nt - 1)

    ring_open(MIX)
    gather_open(*tok_args)

    own_rows = pl.ds(pl.multiple_of(f * blk, blk), blk)
    for source, full in rowed.values():
        full[own_rows, :] = source[...]
    full_merge[f] = merge_w[...]
    full_down[f] = down_w[...]
    toks[t] = tokens[...]
    sig[pl.ds(0, 8), :] = jnp.zeros((8, channels), F32)

    pumps(MIX, 1, half - 1)
    gather_relay(*tok_args)
    pump(MIX, half - 1, True)
    ring_open(FEED)
    gather_close(*tok_args)
    taps = conv_taps[:, pl.ds(pl.multiple_of(t * channels, channels), channels)].astype(F32)

    def rows_of(i):
        return pl.ds(pl.multiple_of(i * tile, tile), tile)

    def norm_tile(i, c):
        rows = rows_of(i)
        squares = jnp.zeros((tile, 1), F32)
        for j in range(nt):
            x = toks[j, rows, :].astype(F32)
            squares += jnp.sum(x * x, axis=1, keepdims=True)
        factor = lax.rsqrt(squares / depth + EPS)
        for j in range(nt):
            x = toks[j, rows, :].astype(F32)
            nrm[rows, pl.ds(j * width, width)] = (x * factor * mixer_gain[j]).astype(BF16)
        return c

    lax.fori_loop(0, tiles, norm_tile, 0)
    ring_close(MIX)

    def project(i, c):
        rows = rows_of(i)
        x = nrm[rows, :]
        outer_s[rows, :] = jnp.dot(x, full_outer[...], preferred_element_type=F32)
        inner = jnp.dot(x, full_inner[...], preferred_element_type=F32)
        value = jnp.dot(x, full_value[...], preferred_element_type=F32)
        sig[pl.ds(pl.multiple_of(i * tile + 8, 8), tile), :] = inner * value
        return c

    lax.fori_loop(0, tiles, project, 0)
    for i in range(tiles):
        r = i * tile
        conv = (
            taps[0:1, :] * sig[r + 6 : r + 6 + tile, :]
            + taps[1:2, :] * sig[r + 7 : r + 7 + tile, :]
            + taps[2:3, :] * sig[r + 8 : r + 8 + tile, :]
        )
        gated = outer_s[r : r + tile, :] * conv
        for h in range(channels // HEAD_DIM):
            g = gated[:, h * HEAD_DIM : (h + 1) * HEAD_DIM]
            level = lax.rsqrt(jnp.mean(g * g, axis=1, keepdims=True) + EPS)
            mixed[r : r + tile, h * HEAD_DIM : (h + 1) * HEAD_DIM] = (g * level).astype(BF16)

    def merge_block(b, c):
        part[b] = jnp.dot(mixed[...], full_merge[b], preferred_element_type=F32).astype(BF16)
        return c

    lax.fori_loop(0, n, merge_block, 0)

    def part_slab(j):
        return part.at[pl.ds(j * bps, bps)]

    for o in offsets:
        slab_copy(part_slab(peer(o)), mrecv.at[o - 1], rs_send, rs_recv, o).start()
    pumps(FEED, 1, half - 1)
    for o in offsets:
        slab_copy(part_slab(peer(o)), mrecv.at[o - 1], rs_send, rs_recv, o).wait()

    def add_tile(received, target):
        def body(i, c):
            rows = rows_of(i)
            for q in range(bps):
                total = part[t * bps + q, rows, :].astype(F32)
                for o in offsets:
                    total += received[o - 1, q, rows, :].astype(F32)
                target[rows, pl.ds(q * cols, cols)] = total.astype(BF16)
            return c

        lax.fori_loop(0, tiles, body, 0)

    add_tile(mrecv, msum)
    gather_open(*sum_args)
    merged[t] = msum[...]
    pump(FEED, half - 1, True)
    ring_open(DOWN)
    gather_relay(*sum_args)
    gather_close(*sum_args)

    def first_tile(i, c):
        rows = rows_of(i)
        squares = jnp.zeros((tile, 1), F32)
        for j in range(nt):
            x = merged[j, rows, :].astype(F32)
            squares += jnp.sum(x * x, axis=1, keepdims=True)
        factor = lax.rsqrt(squares / depth + EPS)
        squares = jnp.zeros((tile, 1), F32)
        for j in range(nt):
            x = merged[j, rows, :].astype(F32)
            y = (toks[j, rows, :].astype(F32) + x * factor * merge_gain[j]).astype(BF16)
            toks[j, rows, :] = y
            y = y.astype(F32)
            squares += jnp.sum(y * y, axis=1, keepdims=True)
        factor = lax.rsqrt(squares / depth + EPS)
        for j in range(nt):
            y = toks[j, rows, :].astype(F32)
            nrm[rows, pl.ds(j * width, width)] = (y * factor * channel_gain[j]).astype(BF16)
        return c

    lax.fori_loop(0, tiles, first_tile, 0)
    ring_close(FEED)

    def feed_tile(i, c):
        rows = rows_of(i)
        x = nrm[rows, :]
        gate = jnp.dot(x, full_gate[...], preferred_element_type=F32)
        upward = jnp.dot(x, full_up[...], preferred_element_type=F32)
        hidden[rows, :] = (gate / (1.0 + jnp.exp(-gate)) * upward).astype(BF16)
        return c

    lax.fori_loop(0, tiles * 3 // 4, feed_tile, 0)
    pump(DOWN, 1)
    lax.fori_loop(tiles * 3 // 4, tiles, feed_tile, 0)

    def down_copy(b):
        j = b // bps
        q = lax.rem(b, bps)
        o = lax.rem(j - t + nt, nt)
        return pltpu.make_async_remote_copy(
            src_ref=part.at[b], dst_ref=drecv.at[o - 1, q],
            send_sem=dn_send.at[b], recv_sem=dn_recv.at[o - 1, q],
            device_id={"tp": j}, device_id_type=MESH,
        )

    def down_block(k):
        b = owner(pos + k)
        part[b] = jnp.dot(hidden[...], full_down[b], preferred_element_type=F32).astype(BF16)

        @pl.when(b // bps != t)
        def _():
            down_copy(b).start()

    def down_pair(s):
        lax.fori_loop(0, 2, lambda i, c: (down_block(s - 2 * s * i), c)[1], 0)

    def down_step(s, c):
        pump(DOWN, s)
        down_pair(s)
        return c

    down_block(0)
    down_pair(1)
    lax.fori_loop(2, half - 1, down_step, 0)
    pump(DOWN, half - 1, True)
    down_pair(half - 1)
    ring_close(DOWN)
    down_block(half)
    for o in offsets:
        for q in range(bps):
            got = drecv.at[o - 1, q]
            pltpu.make_async_remote_copy(
                src_ref=got, dst_ref=got, send_sem=dn_send.at[0], recv_sem=dn_recv.at[o - 1, q],
                device_id={"tp": peer(o)}, device_id_type=MESH,
            ).wait_recv()
    add_tile(drecv, msum)

    def square_tile(i, c):
        rows = rows_of(i)
        x = msum[rows, :].astype(F32)
        sq_own[:, rows] = lax.dot_general(
            jnp.ones((8, width), F32), x * x, (((1,), (1,)), ((), ())),
            precision=lax.Precision.HIGHEST, preferred_element_type=F32,
        )
        return c

    lax.fori_loop(0, tiles, square_tile, 0)
    for o in offsets:
        slab_copy(sq_own, sq_in.at[o - 1], sq_send, sq_recv, o).start()
    for o in offsets:
        for q in range(bps):
            down_copy(peer(o) * bps + q).wait_send()
    for o in offsets:
        slab_copy(sq_own, sq_in.at[o - 1], sq_send, sq_recv, o).wait()

    def last_tile(i, c):
        rows = rows_of(i)
        squares = sq_own[:, rows]
        for o in offsets:
            squares += sq_in[o - 1, :, rows]
        factor = lax.rsqrt(jnp.transpose(squares)[:, 0:1] / depth + EPS)
        y = toks[t, rows, :].astype(F32) + msum[rows, :].astype(F32) * factor * output_gain[t]
        out[rows, :] = y.astype(BF16)
        return c

    lax.fori_loop(0, tiles, last_tile, 0)


def solution(mesh):
    n, nt = mesh.shape["fs"], mesh.shape["tp"]

    def shards(
        tokens, mixer_gain, conv_taps, outer_weight, inner_weight, value_weight, merge_weight,
        merge_gain, channel_gain, gate_weight, up_weight, down_weight, output_gain,
    ):
        length, width = tokens.shape
        blk, channels = outer_weight.shape
        units = gate_weight.shape[1]
        cols = merge_weight.shape[1]
        depth = width * nt
        bps = n // nt
        def slabs(gain):
            return gain.reshape(nt, 1, width)

        vmem = pl.BlockSpec(memory_space=pltpu.VMEM)
        dma = pltpu.SemaphoreType.DMA
        return pl.pallas_call(
            lambda *refs: layer_kernel(n, nt, *refs),
            out_shape=jax.ShapeDtypeStruct((length, width), BF16),
            in_specs=[vmem] * 13,
            out_specs=vmem,
            scratch_shapes=[
                pltpu.VMEM((nt, length, width), BF16),
                pltpu.VMEM((length, depth), BF16),
                pltpu.VMEM((n * blk, channels), BF16),
                pltpu.VMEM((n * blk, channels), BF16),
                pltpu.VMEM((n * blk, channels), BF16),
                pltpu.VMEM((n, channels, cols), BF16),
                pltpu.VMEM((n * blk, units), BF16),
                pltpu.VMEM((n * blk, units), BF16),
                pltpu.VMEM((n, units, cols), BF16),
                pltpu.VMEM((length, channels), F32),
                pltpu.VMEM((length + 8, channels), F32),
                pltpu.VMEM((length, channels), BF16),
                pltpu.VMEM((n, length, cols), BF16),
                pltpu.VMEM((nt - 1, bps, length, cols), BF16),
                pltpu.VMEM((length, width), BF16),
                pltpu.VMEM((nt, length, width), BF16),
                pltpu.VMEM((length, units), BF16),
                pltpu.VMEM((nt - 1, bps, length, cols), BF16),
                pltpu.VMEM((8, length), F32),
                pltpu.VMEM((nt - 1, 8, length), F32),
                dma((2, 2, 8)),
                dma((2, 2, 8, n // 2)),
                dma((nt - 1,)), dma((nt - 1,)),
                dma((nt - 1,)), dma((nt - 1,)),
                dma((nt - 1,)), dma((nt - 1,)),
                dma((n,)), dma((nt - 1, bps)),
                dma((nt - 1,)), dma((nt - 1,)),
            ],
            compiler_params=pltpu.CompilerParams(
                collective_id=0, has_side_effects=True, vmem_limit_bytes=67043328
            ),
        )(
            tokens, slabs(mixer_gain), conv_taps, outer_weight, inner_weight, value_weight,
            merge_weight, slabs(merge_gain), slabs(channel_gain), gate_weight, up_weight,
            down_weight, slabs(output_gain),
        )

    return jax.shard_map(
        shards,
        mesh=mesh,
        in_specs=(
            P("fs", "tp"), P(), P(), P("fs", "tp"), P("fs", "tp"), P("fs", "tp"), P("tp", "fs"),
            P(), P(), P("fs", "tp"), P("fs", "tp"), P("tp", "fs"), P(),
        ),
        out_specs=P("fs", "tp"),
        check_vma=False,
    )
```

profile of v0, /device:TPU:0, one launch (start us, length us, event | category | flops | bytes accessed | tf_op | source)
XLA Modules:
  0.0 249.0 jit_solution(2010159558894322122)
XLA Ops:
  0.0 246.8 %shard_map.127 = bf16[1024,512]{1,0:T(8,128)(2,1)} custom-call(bf16[1024,512]{1,0:T(8,128)(2,1)} %refs_0_.1, f32[4,1,512]{2,1,0:T(1,128)} %bitcast.4, bf16[3,1024]{1,0:T(4,128)(2,1)} %refs_2_.1, bf16[256,256]{1,0:T(8,128)(2,1)} %refs_3_.1, bf16[256,256]{1,0:T(8,128)(2,1)} %refs_4_.1, bf16[256,256]{1,0:T(8,128)(2,1)} %refs_5_.1, bf16[256,256]{1,0:T(8,128)(2,1)} %refs_6_.1, ...), custom_call_target="tpu_custom_call" | custom-call | tf_op jit(solution)/shard_map/pallas_call | solution.py:375
  246.8 2.3 copy.15
where the time goes:
time: 249 us
  Pallas kernels  247 us (99%)
    pallas_call x1, Pallas kernels, shards(): pl.pallas_call(lambda *refs: layer_kernel(n, nt, *refs), out_shape=jax.Sh...  247 us

commit v1 on v0

v1 whole, which is shorter than its diff:
```python
import jax
import jax.numpy as jnp
from jax import lax
from jax.experimental import pallas as pl
from jax.experimental.pallas import tpu as pltpu
from jax.sharding import PartitionSpec as P

HEAD_DIM = 128
EPS = 1e-06
MESH = pl.DeviceIdType.MESH
F32 = jnp.float32
BF16 = jnp.bfloat16
MIX = (0, 1, 2, 3)
GATE, UP, DOWN = 0, 1, 2


def plane_rows(n):
    r = 1
    while 8 * r * r <= n:
        r *= 2
    return r


def layer_kernel(
    n, nt, tokens, mixer_gain, conv_taps, outer_w, inner_w, value_w, merge_w, merge_gain,
    channel_gain, gate_w, up_w, down_w, output_gain,
    out,
    toks, nrm, full_outer, full_inner, full_value, full_merge, full_gate, full_up, full_down,
    outer_s, sig, mixed, part, pa, pc, msum, first, fst, hidden, xr, zr, fr, sq_own, sq_in,
    ring_send, ring_recv, tok_send, tok_recv, pa_send, pa_recv, pc_send, pc_recv,
    z_send, z_recv, y_send, y_recv, d_send, d_recv,
    a_send, a_recv, rl_send, xr_send, xr_recv, zr_send, zr_recv, fr_send, fr_recv,
    sq_send, sq_recv,
):
    f, t = lax.axis_index("fs"), lax.axis_index("tp")
    half = n // 2
    odd = lax.rem(f, 2)
    pos = (1 - odd) * (f // 2) + odd * (n - 1 - f // 2)
    length, width = tokens.shape
    blk, channels = outer_w.shape
    cols = merge_w.shape[1]
    units = gate_w.shape[1]
    bps = n // nt
    depth = width * nt
    tile = min(256, length)
    tiles = length // tile

    yy = plane_rows(n)
    zz = n // yy
    nx = nt // 2
    z, y = f // yy, lax.rem(f, yy)
    x, c = t // 2, lax.rem(t, 2)
    p = lax.rem(z, 2)
    mate = t + 1 - 2 * c
    zpair = z + 1 - 2 * p
    zs = z - p + c
    home = p == c
    away = p != c

    def xor(a, b):
        total, bit = 0, 1
        while bit < zz:
            total = total + lax.rem(a // bit + b // bit, 2) * bit
            bit *= 2
        return total

    def at(zi, yi):
        return zi * yy + yi

    def xat(o):
        return lax.rem(x + o, nx)

    def send(src, dst, ssem, rsem, to):
        return pltpu.make_async_remote_copy(
            src_ref=src, dst_ref=dst, send_sem=ssem, recv_sem=rsem,
            device_id=to, device_id_type=MESH,
        )

    def owner(p):
        q = lax.rem(p + 2 * n, n)
        high = q // half
        return (1 - high) * (2 * q) + high * (2 * (n - 1 - q) + 1)

    right, left = owner(pos + 1), owner(pos - 1)
    rowed = {0: (outer_w, full_outer), 1: (inner_w, full_inner), 2: (value_w, full_value)}
    piece_m = channels // 2

    def own_region(w, h):
        if w in rowed:
            return rowed[w][0].at[pl.ds(h * (blk // 2), blk // 2)]
        return merge_w.at[pl.ds(h * piece_m, piece_m)]

    def region(w, h, p):
        i = owner(p)
        if w in rowed:
            start = pl.multiple_of(i * blk + h * (blk // 2), blk // 2)
            return rowed[w][1].at[pl.ds(start, blk // 2)]
        return full_merge.at[i, pl.ds(h * piece_m, piece_m)]

    def ring_copy(w, h, d, s, first=False):
        dst = region(w, h, pos - s if d == 0 else pos + s)
        return send(
            own_region(w, h) if first else dst, dst, ring_send.at[d, h, w],
            ring_recv.at[d, h, w, s], {"fs": right if d == 0 else left},
        )

    def ring_arrive(w, h, d, s):
        got = region(w, h, pos - 1 - s if d == 0 else pos + 1 + s)
        send(got, got, ring_send.at[d, h, w], ring_recv.at[d, h, w, s],
             {"fs": right if d == 0 else left}).wait_recv()

    def pieces(ws):
        return [(w, (i + d) % 2, d) for i in (0, 1) for w in ws for d in (0, 1)]

    def ring_open(ws):
        for w, h, d in pieces(ws):
            ring_copy(w, h, d, 0, True).start()

    def pump(ws, s, last=False):
        for w, h, d in pieces(ws):
            if last and h != d:
                continue
            ring_arrive(w, h, d, s - 1)
            ring_copy(w, h, d, s - 1).wait_send()
            ring_copy(w, h, d, s).start()
        for w, h, d in pieces(ws):
            if last and h != d:
                ring_arrive(w, h, d, s - 1)
                ring_copy(w, h, d, s - 1).wait_send()

    def pumps(ws, low, high):
        lax.fori_loop(low, high, lambda s, c: (pump(ws, s), c)[1], 0)

    def ring_close(ws):
        for w in ws:
            for d in (0, 1):
                ring_arrive(w, d, d, half - 1)
                ring_copy(w, d, d, half - 1).wait_send()

    def peer(o):
        return lax.rem(t + o, nt)

    offsets = range(1, nt)
    partner = mate
    strides = range(2, nt, 2)

    def hop(src, dst, ssem, rsem, i, to):
        return send(src, dst, ssem.at[i], rsem.at[i], {"tp": to})

    def gather_open(own, held, send, recv):
        for o in strides:
            hop(own, held.at[t], send, recv, o - 1, peer(o)).start()
        hop(own, held.at[t], send, recv, 0, partner).start()

    def gather_relay(own, held, send, recv):
        for o in strides:
            slab = held.at[peer(nt - o)]
            hop(own, slab, send, recv, o - 1, peer(o)).wait()
            hop(slab, slab, send, recv, o, partner).start()

    def gather_close(own, held, send, recv):
        hop(own, held.at[partner], send, recv, 0, partner).wait()
        for o in strides:
            slab = held.at[lax.rem(partner + nt - o, nt)]
            hop(held.at[peer(nt - o)], slab, send, recv, o, partner).wait()

    tok_args = (tokens, toks, tok_send, tok_recv)

    feed_in, feed_full = (gate_w, up_w), (full_gate, full_up)
    hr, hu = blk // 2, units // 2

    def feed_own(w, h):
        if w < DOWN:
            return feed_in[w].at[pl.ds(pl.multiple_of(h * hr, hr), hr)]
        return down_w.at[pl.ds(pl.multiple_of(h * hu, hu), hu)]

    def feed_region(w, g, h):
        if w < DOWN:
            return feed_full[w].at[pl.ds(pl.multiple_of(g * blk + h * hr, hr), hr)]
        return full_down.at[g, pl.ds(pl.multiple_of(h * hu, hu), hu)]

    def z_copies(w):
        for k in range(zz // 2):
            zc = 2 * xor(z // 2, k) + c
            for h in (0, 1):
                copy = send(feed_own(w, h), feed_region(w, f, h), z_send.at[w, k, h],
                            z_recv.at[w, z], {"fs": at(zc, y), "tp": 2 * x + h})
                yield jnp.logical_or(zc != z, c != h), copy

    def y_copies(w, zi, src):
        g = at(zi, y)
        for o in range(1, yy):
            yield send(src, feed_region(w, g, c), y_send.at[w, zi, o - 1], y_recv.at[w, g],
                       {"fs": at(z, lax.rem(y + o, yy))})

    def d_copy(w, g, src):
        return send(src, feed_region(w, g, c), d_send.at[w, g], d_recv.at[w, g], {"tp": mate})

    def feed_open(ws):
        for w in ws:
            @pl.when(home)
            def _():
                for copy in y_copies(w, z, feed_own(w, c)):
                    copy.start()

            for wanted, copy in z_copies(w):
                pl.when(wanted)(copy.start)

            @pl.when(home)
            def _():
                d_copy(w, f, feed_own(w, c)).start()
                if w < DOWN:
                    feed_full[w][pl.ds(pl.multiple_of(f * blk, blk), blk), :] = feed_in[w][...]
                else:
                    full_down[f] = down_w[...]

    def z_arrive(w, zi):
        got = feed_region(w, at(zi, y), c)
        send(got, got, z_send.at[w, 0, 0], z_recv.at[w, zi], {"tp": mate}).wait_recv()
        return got

    def feed_first(w):
        @pl.when(away)
        def _():
            got = z_arrive(w, z)
            for copy in y_copies(w, z, got):
                copy.start()

    def feed_relay(w, o):
        zi = xor(z, o)
        got = z_arrive(w, zi)
        for copy in y_copies(w, zi, got):
            copy.start()
        d_copy(w, at(zi, y), got).start()

    def feed_share(w, o, j):
        g = at(xor(z, o), lax.rem(y + j, yy))
        got = feed_region(w, g, c)
        send(got, got, y_send.at[w, 0, 0], y_recv.at[w, g], {"tp": mate}).wait_recv()
        d_copy(w, g, got).start()

    def feed_shares(w):
        for j in range(1, yy):
            lax.fori_loop(0, zz, lambda o, s: (feed_share(w, o, j), s)[1], 0)

    def d_arrive(w, g):
        got = feed_region(w, g, 1 - c)
        send(got, got, d_send.at[w, g], d_recv.at[w, g], {"tp": mate}).wait_recv()

    def feed_ready(w):
        def body(g, s):
            @pl.when(jnp.logical_or(g != f, away))
            def _():
                d_arrive(w, g)
            return s

        lax.fori_loop(0, n, body, 0)

    def feed_close():
        for w in (GATE, UP, DOWN):
            for wanted, copy in z_copies(w):
                pl.when(wanted)(copy.wait_send)

            def rows_done(zi, s):
                for copy in y_copies(w, zi, feed_own(w, c)):
                    copy.wait_send()
                return s

            def pieces_done(g, s):
                @pl.when(jnp.logical_or(g != f, home))
                def _():
                    d_copy(w, g, feed_own(w, c)).wait_send()
                return s

            lax.fori_loop(0, zz, rows_done, 0)
            lax.fori_loop(0, n, pieces_done, 0)

    barrier = pltpu.get_barrier_semaphore()
    greet = [{"fs": left}, {"fs": right}] + [{"tp": peer(o)} for o in offsets]
    greet += [{"fs": at(z, lax.rem(y + o, yy))} for o in range(1, yy)]
    greet += [{"fs": at(xor(z, o), y), "tp": 2 * x + h} for o in range(1, zz) for h in (0, 1)]
    for to in greet:
        pl.semaphore_signal(barrier, inc=1, device_id=to, device_id_type=MESH)
    pl.semaphore_wait(barrier, len(greet))

    ring_open(MIX)
    gather_open(*tok_args)

    own_rows = pl.ds(pl.multiple_of(f * blk, blk), blk)
    for source, full in rowed.values():
        full[own_rows, :] = source[...]
    full_merge[f] = merge_w[...]
    toks[t] = tokens[...]
    sig[pl.ds(0, 8), :] = jnp.zeros((8, channels), F32)

    pumps(MIX, 1, half - 1)
    gather_relay(*tok_args)
    pump(MIX, half - 1, True)
    feed_open((GATE, UP))
    gather_close(*tok_args)
    taps = conv_taps[:, pl.ds(pl.multiple_of(t * channels, channels), channels)].astype(F32)

    def rows_of(i):
        return pl.ds(pl.multiple_of(i * tile, tile), tile)

    def norm_tile(i, c):
        rows = rows_of(i)
        squares = jnp.zeros((tile, 1), F32)
        for j in range(nt):
            x = toks[j, rows, :].astype(F32)
            squares += jnp.sum(x * x, axis=1, keepdims=True)
        factor = lax.rsqrt(squares / depth + EPS)
        for j in range(nt):
            x = toks[j, rows, :].astype(F32)
            nrm[rows, pl.ds(j * width, width)] = (x * factor * mixer_gain[j]).astype(BF16)
        return c

    lax.fori_loop(0, tiles, norm_tile, 0)
    feed_first(GATE)
    feed_first(UP)
    ring_close(MIX)

    def project(i, c):
        rows = rows_of(i)
        x = nrm[rows, :]
        outer_s[rows, :] = jnp.dot(x, full_outer[...], preferred_element_type=F32)
        inner = jnp.dot(x, full_inner[...], preferred_element_type=F32)
        value = jnp.dot(x, full_value[...], preferred_element_type=F32)
        sig[pl.ds(pl.multiple_of(i * tile + 8, 8), tile), :] = inner * value
        return c

    lax.fori_loop(0, tiles, project, 0)
    for i in range(tiles):
        r = i * tile
        conv = (
            taps[0:1, :] * sig[r + 6 : r + 6 + tile, :]
            + taps[1:2, :] * sig[r + 7 : r + 7 + tile, :]
            + taps[2:3, :] * sig[r + 8 : r + 8 + tile, :]
        )
        gated = outer_s[r : r + tile, :] * conv
        for h in range(channels // HEAD_DIM):
            g = gated[:, h * HEAD_DIM : (h + 1) * HEAD_DIM]
            level = lax.rsqrt(jnp.mean(g * g, axis=1, keepdims=True) + EPS)
            mixed[r : r + tile, h * HEAD_DIM : (h + 1) * HEAD_DIM] = (g * level).astype(BF16)

    def merge_block(b):
        part[b] = jnp.dot(mixed[...], full_merge[b], preferred_element_type=F32).astype(BF16)

    def pair_copy(o, q):
        b = (2 * xat(o) + 1 - c) * bps + q
        return b, send(part.at[b], pa.at[o, q], pa_send.at[o, q], pa_recv.at[o, q], {"tp": mate})

    def pair_send(o, q):
        b, copy = pair_copy(o, q)
        merge_block(b)
        copy.start()

    def cross_copy(o, q):
        b = (2 * xat(o) + c) * bps + q
        return b, send(part.at[b], pc.at[o - 1, q], pc_send.at[o - 1, q], pc_recv.at[o - 1, q],
                       {"tp": 2 * xat(o) + c})

    def add_into(b, others):
        def body(i, s):
            rows = rows_of(i)
            total = part[b, rows, :].astype(F32)
            for other in others:
                total += other[rows, :].astype(F32)
            part[b, rows, :] = total.astype(BF16)
            return s

        lax.fori_loop(0, tiles, body, 0)

    each_block = [(o, q) for o in range(1, nx) for q in range(bps)]
    feed_relay(GATE, 1)
    for o, q in each_block:
        pair_send(o, q)
    for o, q in each_block:
        b, copy = cross_copy(o, q)
        merge_block(b)
        pair_copy(o, q)[1].wait_recv()
        add_into(b, [pa.at[o, q]])
        copy.start()
    for q in range(bps):
        pair_send(0, q)
    for q in range(bps):
        merge_block(t * bps + q)

    lax.fori_loop(2, zz, lambda o, s: (feed_relay(GATE, o), s)[1], 0)
    feed_relay(UP, 1)

    for q in range(bps):
        pair_copy(0, q)[1].wait_recv()
    for o, q in each_block:
        cross_copy(o, q)[1].wait_recv()

    def merged_tile(i, s):
        rows = rows_of(i)
        for q in range(bps):
            total = part[t * bps + q, rows, :].astype(F32) + pa[0, q, rows, :].astype(F32)
            for o in range(1, nx):
                total += pc[o - 1, q, rows, :].astype(F32)
            msum[rows, pl.ds(q * cols, cols)] = total.astype(BF16)
        return s

    lax.fori_loop(0, tiles, merged_tile, 0)

    def square_copy(k, o):
        return send(sq_own.at[k], sq_in.at[k, o - 1], sq_send.at[k, o - 1], sq_recv.at[k, o - 1],
                    {"tp": peer(o)})

    def square_open(k):
        def square_tile(i, c):
            rows = rows_of(i)
            x = msum[rows, :].astype(F32)
            sq_own[k, :, rows] = lax.dot_general(
                jnp.ones((8, width), F32), x * x, (((1,), (1,)), ((), ())),
                precision=lax.Precision.HIGHEST, preferred_element_type=F32,
            )
            return c

        lax.fori_loop(0, tiles, square_tile, 0)
        for o in offsets:
            square_copy(k, o).start()

    def square_close(k):
        for o in offsets:
            square_copy(k, o).wait()

    def level_of(k, rows):
        squares = sq_own[k, :, rows]
        for o in offsets:
            squares += sq_in[k, o - 1, :, rows]
        return lax.rsqrt(jnp.transpose(squares)[:, 0:1] / depth + EPS)

    square_open(0)
    for o in range(nx):
        for q in range(bps):
            pair_copy(o, q)[1].wait_send()
    for o, q in each_block:
        cross_copy(o, q)[1].wait_send()
    square_close(0)

    def slab(tt, r):
        return fst.at[tt, rows_of(r)]

    def first_copies(r):
        src = first.at[rows_of(r)]
        for o in range(1, nx):
            yield None, send(src, slab(t, r), a_send.at[o, r], a_recv.at[t, r],
                             {"tp": 2 * xat(o) + p})
        yield None, send(src, slab(t, r), a_send.at[nx, r], a_recv.at[t, r],
                         {"fs": at(zpair, y), "tp": 2 * x + p})
        yield away, send(src, slab(t, r), a_send.at[0, r], a_recv.at[t, r], {"tp": mate})

    def first_tile(r, s):
        rows = rows_of(r)
        level = level_of(0, rows)
        v = tokens[rows, :].astype(F32) + msum[rows, :].astype(F32) * level * merge_gain[t]
        first[rows, :] = v.astype(BF16)
        for wanted, copy in first_copies(r):
            if wanted is None:
                copy.start()
            else:
                pl.when(wanted)(copy.start)

        @pl.when(home)
        def _():
            fst[t, rows, :] = first[rows, :]
        return s

    lax.fori_loop(0, tiles, first_tile, 0)
    lax.fori_loop(2, zz, lambda o, s: (feed_relay(UP, o), s)[1], 0)
    feed_open((DOWN,))
    feed_first(DOWN)

    def slab_wait(tt, r):
        got = slab(tt, r)
        send(got, got, a_send.at[0, r], a_recv.at[tt, r], {"tp": mate}).wait_recv()
        return got

    def relay_copies(r, got, tt):
        for o in range(1, nx):
            yield send(got, got, rl_send.at[o - 1, r], a_recv.at[tt, r], {"tp": 2 * xat(o) + c})

    def pair_relay(r, got, tt, o):
        return send(got, got, rl_send.at[o - 1, r], a_recv.at[tt, r], {"fs": at(zpair, y)})

    def first_relay(r):
        @pl.when(home)
        def _():
            for o in range(1, nx):
                tt = 2 * xat(o) + 1
                pair_relay(r, slab_wait(tt, r), tt, o).start()

        @pl.when(away)
        def _():
            got = slab_wait(2 * x, r)
            for copy in relay_copies(r, got, 2 * x):
                copy.start()

    def first_rest(r):
        @pl.when(home)
        def _():
            slab_wait(mate, r)
            for o in range(1, nx):
                slab_wait(2 * xat(o), r)

        @pl.when(away)
        def _():
            slab_wait(2 * x + 1, r)
            for o in range(1, nx):
                slab_wait(2 * xat(o), r)
                slab_wait(2 * xat(o) + 1, r)

    def first_done(r, s):
        for wanted, copy in first_copies(r):
            if wanted is None:
                copy.wait_send()
            else:
                pl.when(wanted)(copy.wait_send)
        for copy in relay_copies(r, slab(t, r), t):
            copy.wait_send()
        return s

    def feed_norm(r):
        rows = rows_of(r)
        squares = jnp.zeros((tile, 1), F32)
        for j in range(nt):
            v = fst[j, rows, :].astype(F32)
            squares += jnp.sum(v * v, axis=1, keepdims=True)
        factor = lax.rsqrt(squares / depth + EPS)
        for j in range(nt):
            v = fst[j, rows, :].astype(F32)
            nrm[rows, pl.ds(j * width, width)] = (v * factor * channel_gain[j]).astype(BF16)

    feed_shares(GATE)
    first_relay(0)
    feed_shares(UP)

    def feed_tile(r, s):
        @pl.when(r + 1 < tiles)
        def _():
            first_relay(r + 1)

        first_rest(r)
        feed_norm(r)

        @pl.when(r == 0)
        def _():
            feed_ready(GATE)
            feed_ready(UP)

        rows = rows_of(r)
        v = nrm[rows, :]
        gate = jnp.dot(v, full_gate[...], preferred_element_type=F32)
        upward = jnp.dot(v, full_up[...], preferred_element_type=F32)
        hidden[rows, :] = (gate / (1.0 + jnp.exp(-gate)) * upward).astype(BF16)
        lax.fori_loop(
            1 + r * (zz - 1) // tiles, 1 + (r + 1) * (zz - 1) // tiles,
            lambda o, q: (feed_relay(DOWN, o), q)[1], 0,
        )
        return s

    lax.fori_loop(0, tiles, feed_tile, 0)

    def place(b):
        tt = b // bps
        return tt // 2, lax.rem(tt, 2), lax.rem(b, bps)

    def turn(xt):
        return lax.rem(x - xt + nx, nx)

    def xr_copy(b):
        xt, ct, q = place(b)
        o = turn(xt)
        return send(part.at[b], xr.at[o - 1, q], xr_send.at[b], xr_recv.at[o - 1, q],
                    {"tp": 2 * xt + c})

    def zr_copy(b):
        xt, ct, q = place(b)
        return send(part.at[b], zr.at[xt, q], zr_send.at[b], zr_recv.at[xt, q],
                    {"fs": at(zs, y)})

    def fr_copy(b, i, zt):
        xt, ct, q = place(b)
        return send(part.at[b], fr.at[q, i], fr_send.at[b], fr_recv.at[q, i],
                    {"fs": at(zt, y), "tp": 2 * xt + ct})

    def roles(b):
        xt, ct, q = place(b)
        by_x, mine = ct == 0, xt == x
        other = xt != x
        return {
            "x": (by_x & other, xr_copy(b)),
            "z": ((ct == 1) & away, zr_copy(b)),
            "collect_x": (by_x & mine, None),
            "collect_z": ((ct == 1) & home, None),
            "final_z": (by_x & mine & away, fr_copy(b, 1, zs)),
            "final_x": ((ct == 1) & home & other, fr_copy(b, turn(xt), z)),
            "final_core": (mine & home & (ct != c), fr_copy(b, 0, z)),
            "final_own": (mine & home & (ct == c), None),
        }

    def block_at(k):
        return at(xor(z, lax.rem(k, zz)), lax.rem(y + k // zz, yy))

    def down_block(k, s):
        b = block_at(k)

        @pl.when(k + 1 >= zz)
        def _():
            @pl.when(k + 1 < n)
            def _():
                feed_share(DOWN, lax.rem(k + 1, zz), (k + 1) // zz)

        @pl.when(jnp.logical_or(b != f, away))
        def _():
            d_arrive(DOWN, b)

        part[b] = jnp.dot(hidden[...], full_down[b], preferred_element_type=F32).astype(BF16)
        way = roles(b)
        for key in ("x", "z"):
            wanted, copy = way[key]
            pl.when(wanted)(copy.start)
        return s

    lax.fori_loop(0, n, down_block, 0)

    def collect(k, s):
        b = block_at(k)
        xt, ct, q = place(b)
        way = roles(b)

        @pl.when(way["collect_x"][0])
        def _():
            for o in range(1, nx):
                got = xr.at[o - 1, q]
                send(got, got, xr_send.at[b], xr_recv.at[o - 1, q], {"tp": mate}).wait_recv()
            add_into(b, [xr.at[o - 1, q] for o in range(1, nx)])

        @pl.when(way["collect_z"][0])
        def _():
            got = zr.at[xt, q]
            send(got, got, zr_send.at[b], zr_recv.at[xt, q], {"tp": mate}).wait_recv()
            add_into(b, [zr.at[xt, q]])

        for key in ("final_z", "final_x", "final_core"):
            wanted, copy = way[key]
            pl.when(wanted)(copy.start)

        @pl.when(way["final_own"][0])
        def _():
            fr[q, 0] = part[b]
        return s

    lax.fori_loop(0, n, collect, 0)

    def share_wait(q, i):
        got = fr.at[q, i]
        send(got, got, fr_send.at[0], fr_recv.at[q, i], {"tp": mate}).wait_recv()

    def final_sum(count):
        for q in range(bps):
            pl.when(away)(lambda: share_wait(q, 0))
            for i in range(1, count):
                share_wait(q, i)

            def body(i, s):
                rows = rows_of(i)
                total = fr[q, 0, rows, :].astype(F32)
                for j in range(1, count):
                    total += fr[q, j, rows, :].astype(F32)
                msum[rows, pl.ds(q * cols, cols)] = total.astype(BF16)
                return s

            lax.fori_loop(0, tiles, body, 0)

    if nx == 2:
        final_sum(2)
    else:
        pl.when(c == 0)(lambda: final_sum(2))
        pl.when(c == 1)(lambda: final_sum(nx))

    square_open(1)

    def sent(b, s):
        way = roles(b)
        for key in ("x", "z", "final_z", "final_x", "final_core"):
            wanted, copy = way[key]
            pl.when(wanted)(copy.wait_send)
        return s

    lax.fori_loop(0, n, sent, 0)
    lax.fori_loop(0, tiles, first_done, 0)
    feed_close()
    square_close(1)

    def last_tile(i, c):
        rows = rows_of(i)
        level = level_of(1, rows)
        v = first[rows, :].astype(F32) + msum[rows, :].astype(F32) * level * output_gain[t]
        out[rows, :] = v.astype(BF16)
        return c

    lax.fori_loop(0, tiles, last_tile, 0)


def solution(mesh):
    n, nt = mesh.shape["fs"], mesh.shape["tp"]

    def shards(
        tokens, mixer_gain, conv_taps, outer_weight, inner_weight, value_weight, merge_weight,
        merge_gain, channel_gain, gate_weight, up_weight, down_weight, output_gain,
    ):
        length, width = tokens.shape
        blk, channels = outer_weight.shape
        units = gate_weight.shape[1]
        cols = merge_weight.shape[1]
        depth = width * nt
        bps = n // nt
        nx = nt // 2
        yy = plane_rows(n)
        zz = n // yy
        tiles = length // min(256, length)
        most = max(2, nx)

        def slabs(gain):
            return gain.reshape(nt, 1, width)

        vmem = pl.BlockSpec(memory_space=pltpu.VMEM)
        dma = pltpu.SemaphoreType.DMA
        return pl.pallas_call(
            lambda *refs: layer_kernel(n, nt, *refs),
            out_shape=jax.ShapeDtypeStruct((length, width), BF16),
            in_specs=[vmem] * 13,
            out_specs=vmem,
            scratch_shapes=[
                pltpu.VMEM((nt, length, width), BF16),
                pltpu.VMEM((length, depth), BF16),
                pltpu.VMEM((n * blk, channels), BF16),
                pltpu.VMEM((n * blk, channels), BF16),
                pltpu.VMEM((n * blk, channels), BF16),
                pltpu.VMEM((n, channels, cols), BF16),
                pltpu.VMEM((n * blk, units), BF16),
                pltpu.VMEM((n * blk, units), BF16),
                pltpu.VMEM((n, units, cols), BF16),
                pltpu.VMEM((length, channels), F32),
                pltpu.VMEM((length + 8, channels), F32),
                pltpu.VMEM((length, channels), BF16),
                pltpu.VMEM((n, length, cols), BF16),
                pltpu.VMEM((nx, bps, length, cols), BF16),
                pltpu.VMEM((nx - 1, bps, length, cols), BF16),
                pltpu.VMEM((length, width), BF16),
                pltpu.VMEM((length, width), BF16),
                pltpu.VMEM((nt, length, width), BF16),
                pltpu.VMEM((length, units), BF16),
                pltpu.VMEM((nx - 1, bps, length, cols), BF16),
                pltpu.VMEM((nx, bps, length, cols), BF16),
                pltpu.VMEM((bps, most, length, cols), BF16),
                pltpu.VMEM((2, 8, length), F32),
                pltpu.VMEM((2, nt - 1, 8, length), F32),
                dma((2, 2, 4)),
                dma((2, 2, 4, n // 2)),
                dma((nt - 1,)), dma((nt - 1,)),
                dma((nx, bps)), dma((nx, bps)),
                dma((nx - 1, bps)), dma((nx - 1, bps)),
                dma((3, zz // 2, 2)), dma((3, zz)),
                dma((3, zz, yy - 1)), dma((3, n)),
                dma((3, n)), dma((3, n)),
                dma((nx + 1, tiles)), dma((nt, tiles)), dma((nx - 1, tiles)),
                dma((n,)), dma((nx - 1, bps)),
                dma((n,)), dma((nx, bps)),
                dma((n,)), dma((bps, most)),
                dma((2, nt - 1)), dma((2, nt - 1)),
            ],
            compiler_params=pltpu.CompilerParams(
                collective_id=0, has_side_effects=True, vmem_limit_bytes=67043328
            ),
        )(
            tokens, slabs(mixer_gain), conv_taps, outer_weight, inner_weight, value_weight,
            merge_weight, slabs(merge_gain), slabs(channel_gain), gate_weight, up_weight,
            down_weight, slabs(output_gain),
        )

    return jax.shard_map(
        shards,
        mesh=mesh,
        in_specs=(
            P("fs", "tp"), P(), P(), P("fs", "tp"), P("fs", "tp"), P("fs", "tp"), P("tp", "fs"),
            P(), P(), P("fs", "tp"), P("fs", "tp"), P("tp", "fs"), P(),
        ),
        out_specs=P("fs", "tp"),
        check_vma=False,
    )
```

time: 249 us -> 216 us (0.87)
  Pallas kernels: 247 us -> 212 us
    pallas_call x1, Pallas kernels: 247 us -> 212 us  [shards(): pl.pallas_call(lambda *refs: layer_kernel(n, nt, *refs), out_shape=jax.Sh...]
where the time goes in v1:
time: 216 us; the launch traced here: 214 us
  Pallas kernels  212 us (98%)
  local copies, waits for them, and re-layouts  2.26 us (1%)
    pallas_call x1, Pallas kernels, shards(): pl.pallas_call(lambda *refs: layer_kernel(n, nt, *refs), out_shape=jax.Sh...  212 us

profile of v1, /device:TPU:0, one launch (start us, length us, event | category | flops | bytes accessed | tf_op | source)
XLA Modules:
  0.0 214.0 jit_solution(11372290019916166108)
XLA Ops:
  0.0 211.7 %shard_map.127 = bf16[1024,512]{1,0:T(8,128)(2,1)} custom-call(bf16[1024,512]{1,0:T(8,128)(2,1)} %refs_0_.1, f32[4,1,512]{2,1,0:T(1,128)} %bitcast.4, bf16[3,1024]{1,0:T(4,128)(2,1)} %refs_2_.1, bf16[256,256]{1,0:T(8,128)(2,1)} %refs_3_.1, bf16[256,256]{1,0:T(8,128)(2,1)} %refs_4_.1, bf16[256,256]{1,0:T(8,128)(2,1)} %refs_5_.1, bf16[256,256]{1,0:T(8,128)(2,1)} %refs_6_.1, ...), custom_call_target="tpu_custom_call" | custom-call | tf_op jit(solution)/shard_map/pallas_call | solution.py:733
  211.8 2.3 %copy.15 = bf16[1024,512]{1,0:T(8,128)(2,1)} copy(bf16[1024,512]{1,0:T(8,128)(2,1)} %shard_map.127) | data formatting | bytes 2097152

commit v2 on v1

--- a/solution.py
+++ b/solution.py
@@ -1,3 +1,5 @@
+import functools
+
 import jax
 import jax.numpy as jnp
 from jax import lax
@@ -12,6 +14,9 @@
 BF16 = jnp.bfloat16
 MIX = (0, 1, 2, 3)
 GATE, UP, DOWN = 0, 1, 2
+ZSHARE = 0
+XSHARE = 4
+DPLAN = ((1,), (), (2, 3))
 
 
 def plane_rows(n):
@@ -179,13 +184,34 @@
             return feed_full[w].at[pl.ds(pl.multiple_of(g * blk + h * hr, hr), hr)]
         return full_down.at[g, pl.ds(pl.multiple_of(h * hu, hu), hu)]
 
-    def z_copies(w):
+    OWN, INNER, OUTER, FAR = (0,), (1,), (2,), (3,)
+
+    def z_copies(w, kinds=(0, 1, 2, 3)):
         for k in range(zz // 2):
-            zc = 2 * xor(z // 2, k) + c
+            pair = xor(z // 2, k)
+            zc = 2 * pair + c
+            up = (pair > z // 2).astype(jnp.int32)
+            kind = 1 + (c == up).astype(jnp.int32)
+            kind = jnp.where(p == up, kind, 3) if k else 0
             for h in (0, 1):
                 copy = send(feed_own(w, h), feed_region(w, f, h), z_send.at[w, k, h],
                             z_recv.at[w, z], {"fs": at(zc, y), "tp": 2 * x + h})
-                yield jnp.logical_or(zc != z, c != h), copy
+                if k == 0:
+                    if 0 in kinds:
+                        yield jnp.logical_or(zc != z, c != h), copy
+                elif len(kinds) == 4:
+                    yield None, copy
+                else:
+                    wanted = [kind == v for v in kinds if v]
+                    if wanted:
+                        yield functools.reduce(jnp.logical_or, wanted), copy
+
+    def line_at(i):
+        pair = xor(z // 2, i // 2)
+        up = (pair > z // 2).astype(jnp.int32)
+        own = 1 - jnp.minimum(i // 2, 1)
+        begin = own * p + (1 - own) * (1 - up)
+        return 2 * pair + begin + lax.rem(i, 2) * (1 - 2 * begin)
 
     def y_copies(w, zi, src):
         g = at(zi, y)
@@ -195,6 +221,23 @@
 
     def d_copy(w, g, src):
         return send(src, feed_region(w, g, c), d_send.at[w, g], d_recv.at[w, g], {"tp": mate})
+
+    def start(copies):
+        for wanted, copy in copies:
+            if wanted is None:
+                copy.start()
+            else:
+                pl.when(wanted)(copy.start)
+
+    def finish(copies):
+        for wanted, copy in copies:
+            if wanted is None:
+                copy.wait_send()
+            else:
+                pl.when(wanted)(copy.wait_send)
+
+    def feed_cross(w, kinds):
+        start(z_copies(w, kinds))
 
     def feed_open(ws):
         for w in ws:
@@ -202,12 +245,6 @@
             def _():
                 for copy in y_copies(w, z, feed_own(w, c)):
                     copy.start()
-
-            for wanted, copy in z_copies(w):
-                pl.when(wanted)(copy.start)
-
-            @pl.when(home)
-            def _():
                 d_copy(w, f, feed_own(w, c)).start()
                 if w < DOWN:
                     feed_full[w][pl.ds(pl.multiple_of(f * blk, blk), blk), :] = feed_in[w][...]
@@ -227,14 +264,17 @@
                 copy.start()
 
     def feed_relay(w, o):
-        zi = xor(z, o)
+        zi = line_at(o)
         got = z_arrive(w, zi)
         for copy in y_copies(w, zi, got):
             copy.start()
         d_copy(w, at(zi, y), got).start()
 
+    def feed_relays(w, low, high):
+        lax.fori_loop(low, high, lambda o, s: (feed_relay(w, o), s)[1], 0)
+
     def feed_share(w, o, j):
-        g = at(xor(z, o), lax.rem(y + j, yy))
+        g = at(line_at(o), lax.rem(y + j, yy))
         got = feed_region(w, g, c)
         send(got, got, y_send.at[w, 0, 0], y_recv.at[w, g], {"tp": mate}).wait_recv()
         d_copy(w, g, got).start()
@@ -258,8 +298,7 @@
 
     def feed_close():
         for w in (GATE, UP, DOWN):
-            for wanted, copy in z_copies(w):
-                pl.when(wanted)(copy.wait_send)
+            finish(z_copies(w))
 
             def rows_done(zi, s):
                 for copy in y_copies(w, zi, feed_own(w, c)):
@@ -296,6 +335,9 @@
     pumps(MIX, 1, half - 1)
     gather_relay(*tok_args)
     pump(MIX, half - 1, True)
+    feed_cross(GATE, OWN + INNER + OUTER)
+    feed_cross(UP, OWN)
+    feed_cross(DOWN, OWN)
     feed_open((GATE, UP))
     gather_close(*tok_args)
     taps = conv_taps[:, pl.ds(pl.multiple_of(t * channels, channels), channels)].astype(F32)
@@ -372,7 +414,6 @@
         lax.fori_loop(0, tiles, body, 0)
 
     each_block = [(o, q) for o in range(1, nx) for q in range(bps)]
-    feed_relay(GATE, 1)
     for o, q in each_block:
         pair_send(o, q)
     for o, q in each_block:
@@ -386,40 +427,35 @@
     for q in range(bps):
         merge_block(t * bps + q)
 
-    lax.fori_loop(2, zz, lambda o, s: (feed_relay(GATE, o), s)[1], 0)
+    feed_cross(GATE, FAR)
+    feed_cross(UP, INNER + OUTER + FAR)
+    feed_relay(GATE, 1)
     feed_relay(UP, 1)
+    feed_open((DOWN,))
+    feed_first(DOWN)
 
     for q in range(bps):
         pair_copy(0, q)[1].wait_recv()
     for o, q in each_block:
         cross_copy(o, q)[1].wait_recv()
 
-    def merged_tile(i, s):
-        rows = rows_of(i)
-        for q in range(bps):
-            total = part[t * bps + q, rows, :].astype(F32) + pa[0, q, rows, :].astype(F32)
-            for o in range(1, nx):
-                total += pc[o - 1, q, rows, :].astype(F32)
-            msum[rows, pl.ds(q * cols, cols)] = total.astype(BF16)
-        return s
-
-    lax.fori_loop(0, tiles, merged_tile, 0)
-
     def square_copy(k, o):
         return send(sq_own.at[k], sq_in.at[k, o - 1], sq_send.at[k, o - 1], sq_recv.at[k, o - 1],
                     {"tp": peer(o)})
 
+    def squares_of(v):
+        v = v.astype(F32)
+        sq = v * v
+        high = sq.astype(BF16)
+        low = (sq - high.astype(F32)).astype(BF16)
+        ones = jnp.ones((8, sq.shape[1]), BF16)
+        dims = (((1,), (1,)), ((), ()))
+        return (
+            lax.dot_general(ones, high, dims, preferred_element_type=F32)
+            + lax.dot_general(ones, low, dims, preferred_element_type=F32)
+        )
+
     def square_open(k):
-        def square_tile(i, c):
-            rows = rows_of(i)
-            x = msum[rows, :].astype(F32)
-            sq_own[k, :, rows] = lax.dot_general(
-                jnp.ones((8, width), F32), x * x, (((1,), (1,)), ((), ())),
-                precision=lax.Precision.HIGHEST, preferred_element_type=F32,
-            )
-            return c
-
-        lax.fori_loop(0, tiles, square_tile, 0)
         for o in offsets:
             square_copy(k, o).start()
 
@@ -432,6 +468,21 @@
         for o in offsets:
             squares += sq_in[k, o - 1, :, rows]
         return lax.rsqrt(jnp.transpose(squares)[:, 0:1] / depth + EPS)
+
+    def merged_tile(i, s):
+        rows = rows_of(i)
+        squares = jnp.zeros((8, tile), F32)
+        for q in range(bps):
+            total = part[t * bps + q, rows, :].astype(F32) + pa[0, q, rows, :].astype(F32)
+            for o in range(1, nx):
+                total += pc[o - 1, q, rows, :].astype(F32)
+            total = total.astype(BF16)
+            msum[rows, pl.ds(q * cols, cols)] = total
+            squares += squares_of(total)
+        sq_own[0, :, rows] = squares
+        return s
+
+    lax.fori_loop(0, tiles, merged_tile, 0)
 
     square_open(0)
     for o in range(nx):
@@ -458,11 +509,7 @@
         level = level_of(0, rows)
         v = tokens[rows, :].astype(F32) + msum[rows, :].astype(F32) * level * merge_gain[t]
         first[rows, :] = v.astype(BF16)
-        for wanted, copy in first_copies(r):
-            if wanted is None:
-                copy.start()
-            else:
-                pl.when(wanted)(copy.start)
+        start(first_copies(r))
 
         @pl.when(home)
         def _():
@@ -470,24 +517,23 @@
         return s
 
     lax.fori_loop(0, tiles, first_tile, 0)
-    lax.fori_loop(2, zz, lambda o, s: (feed_relay(UP, o), s)[1], 0)
-    feed_open((DOWN,))
-    feed_first(DOWN)
-
     def slab_wait(tt, r):
         got = slab(tt, r)
         send(got, got, a_send.at[0, r], a_recv.at[tt, r], {"tp": mate}).wait_recv()
         return got
 
-    def relay_copies(r, got, tt):
+    by_z = tiles * ZSHARE // 4
+
+    def relay_copies(r, got, tt, k):
         for o in range(1, nx):
-            yield send(got, got, rl_send.at[o - 1, r], a_recv.at[tt, r], {"tp": 2 * xat(o) + c})
+            yield send(got, got, rl_send.at[k, o - 1, r], a_recv.at[tt, r],
+                       {"tp": 2 * xat(o) + c})
 
     def pair_relay(r, got, tt, o):
-        return send(got, got, rl_send.at[o - 1, r], a_recv.at[tt, r], {"fs": at(zpair, y)})
+        return send(got, got, rl_send.at[1, o - 1, r], a_recv.at[tt, r], {"fs": at(zpair, y)})
 
     def first_relay(r):
-        @pl.when(home)
+        @pl.when(jnp.logical_and(home, r < by_z))
         def _():
             for o in range(1, nx):
                 tt = 2 * xat(o) + 1
@@ -496,7 +542,13 @@
         @pl.when(away)
         def _():
             got = slab_wait(2 * x, r)
-            for copy in relay_copies(r, got, 2 * x):
+            for copy in relay_copies(r, got, 2 * x, 0):
+                copy.start()
+
+        @pl.when(jnp.logical_and(away, r >= by_z))
+        def _():
+            got = slab_wait(2 * x + 1, r)
+            for copy in relay_copies(r, got, 2 * x + 1, 1):
                 copy.start()
 
     def first_rest(r):
@@ -506,21 +558,32 @@
             for o in range(1, nx):
                 slab_wait(2 * xat(o), r)
 
+        @pl.when(jnp.logical_and(home, r >= by_z))
+        def _():
+            for o in range(1, nx):
+                slab_wait(2 * xat(o) + 1, r)
+
+        @pl.when(jnp.logical_and(away, r < by_z))
+        def _():
+            slab_wait(2 * x + 1, r)
+
         @pl.when(away)
         def _():
-            slab_wait(2 * x + 1, r)
             for o in range(1, nx):
                 slab_wait(2 * xat(o), r)
                 slab_wait(2 * xat(o) + 1, r)
 
     def first_done(r, s):
-        for wanted, copy in first_copies(r):
-            if wanted is None:
+        finish(first_copies(r))
+        @pl.when(away)
+        def _():
+            for copy in relay_copies(r, slab(t, r), t, 0):
                 copy.wait_send()
-            else:
-                pl.when(wanted)(copy.wait_send)
-        for copy in relay_copies(r, slab(t, r), t):
-            copy.wait_send()
+
+        @pl.when(away == (r >= by_z))
+        def _():
+            for copy in relay_copies(r, slab(t, r), t, 1):
+                copy.wait_send()
         return s
 
     def feed_norm(r):
@@ -534,14 +597,25 @@
             v = fst[j, rows, :].astype(F32)
             nrm[rows, pl.ds(j * width, width)] = (v * factor * channel_gain[j]).astype(BF16)
 
+    DFIRST, DMIDDLE, DLATER = DPLAN
+    feed_relays(GATE, 2, zz)
+    feed_relay(DOWN, 1)
+    first_relay(0)
+    feed_cross(DOWN, DFIRST)
+    feed_relays(UP, 2, zz)
+    first_relay(1)
+    feed_cross(DOWN, DMIDDLE)
     feed_shares(GATE)
-    first_relay(0)
     feed_shares(UP)
 
     def feed_tile(r, s):
-        @pl.when(r + 1 < tiles)
-        def _():
-            first_relay(r + 1)
+        @pl.when(r + 2 < tiles)
+        def _():
+            first_relay(r + 2)
+
+        @pl.when(r == 0)
+        def _():
+            feed_cross(DOWN, DLATER)
 
         first_rest(r)
         feed_norm(r)
@@ -556,10 +630,6 @@
         gate = jnp.dot(v, full_gate[...], preferred_element_type=F32)
         upward = jnp.dot(v, full_up[...], preferred_element_type=F32)
         hidden[rows, :] = (gate / (1.0 + jnp.exp(-gate)) * upward).astype(BF16)
-        lax.fori_loop(
-            1 + r * (zz - 1) // tiles, 1 + (r + 1) * (zz - 1) // tiles,
-            lambda o, q: (feed_relay(DOWN, o), q)[1], 0,
-        )
         return s
 
     lax.fori_loop(0, tiles, feed_tile, 0)
@@ -568,13 +638,16 @@
         tt = b // bps
         return tt // 2, lax.rem(tt, 2), lax.rem(b, bps)
 
+    def first_x(ct, q):
+        return ct * bps + q < 2 * bps * XSHARE // 8
+
     def turn(xt):
         return lax.rem(x - xt + nx, nx)
 
     def xr_copy(b):
         xt, ct, q = place(b)
         o = turn(xt)
-        return send(part.at[b], xr.at[o - 1, q], xr_send.at[b], xr_recv.at[o - 1, q],
+        return send(part.at[b], xr.at[o - 1, ct, q], xr_send.at[b], xr_recv.at[o - 1, ct, q],
                     {"tp": 2 * xt + c})
 
     def zr_copy(b):
@@ -589,24 +662,29 @@
 
     def roles(b):
         xt, ct, q = place(b)
-        by_x, mine = ct == 0, xt == x
+        by_x, mine = first_x(ct, q), xt == x
+        by_z = jnp.logical_not(by_x)
         other = xt != x
         return {
             "x": (by_x & other, xr_copy(b)),
-            "z": ((ct == 1) & away, zr_copy(b)),
+            "z": (by_z & away, zr_copy(b)),
             "collect_x": (by_x & mine, None),
-            "collect_z": ((ct == 1) & home, None),
+            "collect_z": (by_z & home, None),
             "final_z": (by_x & mine & away, fr_copy(b, 1, zs)),
-            "final_x": ((ct == 1) & home & other, fr_copy(b, turn(xt), z)),
+            "final_x": (by_z & home & other, fr_copy(b, turn(xt), z)),
             "final_core": (mine & home & (ct != c), fr_copy(b, 0, z)),
             "final_own": (mine & home & (ct == c), None),
         }
 
     def block_at(k):
-        return at(xor(z, lax.rem(k, zz)), lax.rem(y + k // zz, yy))
+        return at(line_at(lax.rem(k, zz)), lax.rem(y + k // zz, yy))
 
     def down_block(k, s):
         b = block_at(k)
+
+        @pl.when(jnp.logical_and(k >= 1, k + 1 < zz))
+        def _():
+            feed_relay(DOWN, k + 1)
 
         @pl.when(k + 1 >= zz)
         def _():
@@ -635,9 +713,9 @@
         @pl.when(way["collect_x"][0])
         def _():
             for o in range(1, nx):
-                got = xr.at[o - 1, q]
-                send(got, got, xr_send.at[b], xr_recv.at[o - 1, q], {"tp": mate}).wait_recv()
-            add_into(b, [xr.at[o - 1, q] for o in range(1, nx)])
+                got = xr.at[o - 1, ct, q]
+                send(got, got, xr_send.at[b], xr_recv.at[o - 1, ct, q], {"tp": mate}).wait_recv()
+            add_into(b, [xr.at[o - 1, ct, q] for o in range(1, nx)])
 
         @pl.when(way["collect_z"][0])
         def _():
@@ -660,27 +738,32 @@
         got = fr.at[q, i]
         send(got, got, fr_send.at[0], fr_recv.at[q, i], {"tp": mate}).wait_recv()
 
-    def final_sum(count):
-        for q in range(bps):
-            pl.when(away)(lambda: share_wait(q, 0))
-            for i in range(1, count):
-                share_wait(q, i)
-
-            def body(i, s):
-                rows = rows_of(i)
-                total = fr[q, 0, rows, :].astype(F32)
-                for j in range(1, count):
-                    total += fr[q, j, rows, :].astype(F32)
-                msum[rows, pl.ds(q * cols, cols)] = total.astype(BF16)
-                return s
-
-            lax.fori_loop(0, tiles, body, 0)
-
-    if nx == 2:
-        final_sum(2)
-    else:
-        pl.when(c == 0)(lambda: final_sum(2))
-        pl.when(c == 1)(lambda: final_sum(nx))
+    def final_sum(q, count):
+        pl.when(away)(lambda: share_wait(q, 0))
+        for i in range(1, count):
+            share_wait(q, i)
+
+        def body(i, s):
+            rows = rows_of(i)
+            total = fr[q, 0, rows, :].astype(F32)
+            for j in range(1, count):
+                total += fr[q, j, rows, :].astype(F32)
+            total = total.astype(BF16)
+            msum[rows, pl.ds(q * cols, cols)] = total
+            if q:
+                sq_own[1, :, rows] += squares_of(total)
+            else:
+                sq_own[1, :, rows] = squares_of(total)
+            return s
+
+        lax.fori_loop(0, tiles, body, 0)
+
+    for q in range(bps):
+        if nx == 2:
+            final_sum(q, 2)
+        else:
+            pl.when(first_x(c, q))(lambda: final_sum(q, 2))
+            pl.when(jnp.logical_not(first_x(c, q)))(lambda: final_sum(q, nx))
 
     square_open(1)
 
@@ -755,7 +838,7 @@
                 pltpu.VMEM((length, width), BF16),
                 pltpu.VMEM((nt, length, width), BF16),
                 pltpu.VMEM((length, units), BF16),
-                pltpu.VMEM((nx - 1, bps, length, cols), BF16),
+                pltpu.VMEM((nx - 1, 2, bps, length, cols), BF16),
                 pltpu.VMEM((nx, bps, length, cols), BF16),
                 pltpu.VMEM((bps, most, length, cols), BF16),
                 pltpu.VMEM((2, 8, length), F32),
@@ -768,8 +851,8 @@
                 dma((3, zz // 2, 2)), dma((3, zz)),
                 dma((3, zz, yy - 1)), dma((3, n)),
                 dma((3, n)), dma((3, n)),
-                dma((nx + 1, tiles)), dma((nt, tiles)), dma((nx - 1, tiles)),
-                dma((n,)), dma((nx - 1, bps)),
+                dma((nx + 1, tiles)), dma((nt, tiles)), dma((2, nx - 1, tiles)),
+                dma((n,)), dma((nx - 1, 2, bps)),
                 dma((n,)), dma((nx, bps)),
                 dma((n,)), dma((bps, most)),
                 dma((2, nt - 1)), dma((2, nt - 1)),

time: 216 us -> 199 us (0.921)
  Pallas kernels: 212 us -> 196 us
    pallas_call x1, Pallas kernels: 212 us -> 196 us  [shards(): pl.pallas_call(lambda *refs: layer_kernel(n, nt, *refs), out_shape=jax.Sh...]
where the time goes in v2:
time: 199 us; the launch traced here: 198 us
  Pallas kernels  196 us (98%)
  local copies, waits for them, and re-layouts  2.26 us (1%)
    pallas_call x1, Pallas kernels, shards(): pl.pallas_call(lambda *refs: layer_kernel(n, nt, *refs), out_shape=jax.Sh...  196 us

profile of v2, /device:TPU:0, one launch (start us, length us, event | category | flops | bytes accessed | tf_op | source)
XLA Modules:
  0.0 197.9 jit_solution(458099773197249037)
XLA Ops:
  0.0 195.7 %shard_map.127 = bf16[1024,512]{1,0:T(8,128)(2,1)} custom-call(bf16[1024,512]{1,0:T(8,128)(2,1)} %refs_0_.1, f32[4,1,512]{2,1,0:T(1,128)} %bitcast.4, bf16[3,1024]{1,0:T(4,128)(2,1)} %refs_2_.1, bf16[256,256]{1,0:T(8,128)(2,1)} %refs_3_.1, bf16[256,256]{1,0:T(8,128)(2,1)} %refs_4_.1, bf16[256,256]{1,0:T(8,128)(2,1)} %refs_5_.1, bf16[256,256]{1,0:T(8,128)(2,1)} %refs_6_.1, ...), custom_call_target="tpu_custom_call" | custom-call | tf_op jit(solution)/shard_map/pallas_call | solution.py:816
  195.7 2.3 %copy.15 = bf16[1024,512]{1,0:T(8,128)(2,1)} copy(bf16[1024,512]{1,0:T(8,128)(2,1)} %shard_map.127) | data formatting | bytes 2097152

commit v3 on v2

--- a/solution.py
+++ b/solution.py
@@ -35,7 +35,7 @@
     ring_send, ring_recv, tok_send, tok_recv, pa_send, pa_recv, pc_send, pc_recv,
     z_send, z_recv, y_send, y_recv, d_send, d_recv,
     a_send, a_recv, rl_send, xr_send, xr_recv, zr_send, zr_recv, fr_send, fr_recv,
-    sq_send, sq_recv,
+    sq_send, sq_recv, own_sem,
 ):
     f, t = lax.axis_index("fs"), lax.axis_index("tp")
     half = n // 2
@@ -239,6 +239,12 @@
     def feed_cross(w, kinds):
         start(z_copies(w, kinds))
 
+    def feed_here(w):
+        if w < DOWN:
+            held = feed_full[w].at[pl.ds(pl.multiple_of(f * blk, blk), blk)]
+            return pltpu.make_async_copy(feed_in[w], held, own_sem.at[w])
+        return pltpu.make_async_copy(down_w, full_down.at[f], own_sem.at[w])
+
     def feed_open(ws):
         for w in ws:
             @pl.when(home)
@@ -246,10 +252,7 @@
                 for copy in y_copies(w, z, feed_own(w, c)):
                     copy.start()
                 d_copy(w, f, feed_own(w, c)).start()
-                if w < DOWN:
-                    feed_full[w][pl.ds(pl.multiple_of(f * blk, blk), blk), :] = feed_in[w][...]
-                else:
-                    full_down[f] = down_w[...]
+                feed_here(w).start()
 
     def z_arrive(w, zi):
         got = feed_region(w, at(zi, y), c)
@@ -326,9 +329,12 @@
     gather_open(*tok_args)
 
     own_rows = pl.ds(pl.multiple_of(f * blk, blk), blk)
-    for source, full in rowed.values():
-        full[own_rows, :] = source[...]
-    full_merge[f] = merge_w[...]
+    mix_own = [
+        pltpu.make_async_copy(source, full.at[own_rows], own_sem.at[3 + w])
+        for w, (source, full) in rowed.items()
+    ] + [pltpu.make_async_copy(merge_w, full_merge.at[f], own_sem.at[6])]
+    for copy in mix_own:
+        copy.start()
     toks[t] = tokens[...]
     sig[pl.ds(0, 8), :] = jnp.zeros((8, channels), F32)
 
@@ -361,6 +367,8 @@
     feed_first(GATE)
     feed_first(UP)
     ring_close(MIX)
+    for copy in mix_own:
+        copy.wait()
 
     def project(i, c):
         rows = rows_of(i)
@@ -624,6 +632,11 @@
         def _():
             feed_ready(GATE)
             feed_ready(UP)
+
+            @pl.when(home)
+            def _():
+                for w in (GATE, UP, DOWN):
+                    feed_here(w).wait()
 
         rows = rows_of(r)
         v = nrm[rows, :]
@@ -812,11 +825,12 @@
             return gain.reshape(nt, 1, width)
 
         vmem = pl.BlockSpec(memory_space=pltpu.VMEM)
+        held = pl.BlockSpec(memory_space=pl.ANY)
         dma = pltpu.SemaphoreType.DMA
         return pl.pallas_call(
             lambda *refs: layer_kernel(n, nt, *refs),
             out_shape=jax.ShapeDtypeStruct((length, width), BF16),
-            in_specs=[vmem] * 13,
+            in_specs=[vmem] * 3 + [held] * 4 + [vmem] * 2 + [held] * 3 + [vmem],
             out_specs=vmem,
             scratch_shapes=[
                 pltpu.VMEM((nt, length, width), BF16),
@@ -855,7 +869,7 @@
                 dma((n,)), dma((nx - 1, 2, bps)),
                 dma((n,)), dma((nx, bps)),
                 dma((n,)), dma((bps, most)),
-                dma((2, nt - 1)), dma((2, nt - 1)),
+                dma((2, nt - 1)), dma((2, nt - 1)), dma((7,)),
             ],
             compiler_params=pltpu.CompilerParams(
                 collective_id=0, has_side_effects=True, vmem_limit_bytes=67043328

time: 199 us -> 197 us (0.990)
  no operation moved by 1% of the time
where the time goes in v3:
time: 197 us
  Pallas kernels  195 us (99%)
  local copies, waits for them, and re-layouts  2.26 us (1%)
    pallas_call x1, Pallas kernels, shards(): pl.pallas_call(lambda *refs: layer_kernel(n, nt, *refs), out_shape=jax.Sh...  195 us

profile of v3, /device:TPU:0, one launch (start us, length us, event | category | flops | bytes accessed | tf_op | source)
XLA Modules:
  0.0 197.2 jit_solution(6300244072885477086)
XLA Ops:
  0.0 195.0 %shard_map.127 = bf16[1024,512]{1,0:T(8,128)(2,1)} custom-call(bf16[1024,512]{1,0:T(8,128)(2,1)} %refs_0_.1, f32[4,1,512]{2,1,0:T(1,128)} %bitcast.4, bf16[3,1024]{1,0:T(4,128)(2,1)} %refs_2_.1, bf16[256,256]{1,0:T(8,128)(2,1)} %refs_3_.1, bf16[256,256]{1,0:T(8,128)(2,1)} %refs_4_.1, bf16[256,256]{1,0:T(8,128)(2,1)} %refs_5_.1, bf16[256,256]{1,0:T(8,128)(2,1)} %refs_6_.1, ...), custom_call_target="tpu_custom_call" | custom-call | tf_op jit(solution)/shard_map/pallas_call | solution.py:830
  195.0 2.3 %copy.15 = bf16[1024,512]{1,0:T(8,128)(2,1)} copy(bf16[1024,512]{1,0:T(8,128)(2,1)} %shard_map.127) | data formatting | bytes 2097152
